TPU v7x, 256 devices: a whole 4x4x8 slice. The times are simulated.
256 devices in a mesh: ep: 16 (over y, x), tp: 16 (over z, core).
Axes of the slice: x: 4, y: 4, z: 8, core: 2. Of those that a mesh axis runs over, the one named last changes fastest.
Arguments:
- mix_tokens: bfloat16 [32768, 2048], P(('ep', 'tp')), may hold values from -6 to 6
- mix_gain: bfloat16 [2048], replicated, may hold values from 0.099609375 to 1.8984375
- gate_proj: bfloat16 [2048, 1024], P(None, 'tp'), may hold values from -0.125 to 0.125
- conv_proj: bfloat16 [2048, 1024], P(None, 'tp'), may hold values from -0.125 to 0.125
- value_proj: bfloat16 [2048, 1024], P(None, 'tp'), may hold values from -0.125 to 0.125
- conv_taps: bfloat16 [3, 1024], P(None, 'tp'), may hold values from -3 to 3
- out_proj: bfloat16 [1024, 2048], P('tp'), may hold values from -0.1875 to 0.1875
- moe_tokens: bfloat16 [16384, 2048], P(('ep', 'tp')), may hold values from -6 to 6
- moe_gain: bfloat16 [2048], replicated, may hold values from 0.099609375 to 1.8984375
- expert_ids: int32 [16384, 2], P(('ep', 'tp')), may hold values from 0 to 15, all different within a row; in each aligned block of 64 rows (0 to 63, 64 to 127, ...) at most 9 rows name the same one
- expert_scores: float32 [16384, 2], P(('ep', 'tp')), may hold values from -6 to 6
- expert_gate: bfloat16 [16, 2048, 4096], P('ep', None, 'tp'), may hold values from -0.125 to 0.125
- expert_up: bfloat16 [16, 2048, 4096], P('ep', None, 'tp'), may hold values from -0.125 to 0.125
- expert_down: bfloat16 [16, 4096, 2048], P('ep', 'tp'), may hold values from -0.09375 to 0.09375
Outputs:
- mix_out: bfloat16 [32768, 2048], P(('ep', 'tp'))
- moe_out: bfloat16 [16384, 2048], P(('ep', 'tp'))
Inputs may be any that keep to these rules, and one draw needn't show every extreme that they name: `expert_ids`: each row names 2 different experts; among the rows of one device no expert is named more than 9 times.
All inputs are finite; a program needn't handle non-finite values.
Results may differ from a plain program's by a relative error of at most 0.018.
Values may be sent and summed in bfloat16 or wider, within the bound.
A program may use at most 128 MiB of HBM per device.

v0:
```python
import jax
import jax.numpy as jnp
from jax import lax
from jax.sharding import PartitionSpec as P

norm_eps = 1e-06


def from_behind(value, axis, steps):
    count = lax.axis_size(axis)
    leading, last = (max(0, -steps), min(count, count - steps))
    return lax.ppermute(value, axis, [(source, source + steps) for source in range(leading, last)])


def scaled_norm(row_data, gain_vec):
    values = row_data.astype(jnp.float32)
    inverse = lax.rsqrt(jnp.mean(values * values, axis=1, keepdims=True) + norm_eps)
    return (values * inverse * gain_vec.astype(jnp.float32)).astype(jnp.bfloat16)


def shards(
    mix_tokens,
    mix_gain,
    gate_proj,
    conv_proj,
    value_proj,
    conv_taps,
    out_proj,
    moe_tokens,
    moe_gain,
    expert_ids,
    expert_scores,
    expert_gate,
    expert_up,
    expert_down,
):
    normed = scaled_norm(mix_tokens, mix_gain)
    w_joint = jnp.concatenate([gate_proj, conv_proj, value_proj], axis=1)
    combined = jnp.dot(
        lax.all_gather(normed, "tp", axis=0, tiled=True),
        w_joint,
        preferred_element_type=jnp.float32,
    ).astype(jnp.bfloat16)
    channels = gate_proj.shape[1]
    out_gate = combined[:, :channels]
    in_gate = combined[:, channels : 2 * channels]
    values = combined[:, 2 * channels :]
    signal = (in_gate.astype(jnp.float32) * values.astype(jnp.float32)).astype(jnp.bfloat16)
    tap_count = conv_taps.shape[0]
    before = from_behind(signal[signal.shape[0] - (tap_count - 1) :], "ep", 1)
    extended = jnp.concatenate([before, signal], axis=0)
    length = signal.shape[0]
    tap_values = conv_taps.astype(jnp.float32)
    convolved = jnp.zeros((length, channels), jnp.float32)
    for offset in range(tap_count):
        convolved = (
            convolved + extended[offset : offset + length].astype(jnp.float32) * tap_values[offset]
        )
    carried = (out_gate.astype(jnp.float32) * convolved).astype(jnp.bfloat16)
    token_major = lax.all_to_all(carried, "tp", split_axis=0, concat_axis=1, tiled=True)
    mix_out = jnp.dot(
        token_major,
        lax.all_gather(out_proj, "tp", axis=0, tiled=True),
        preferred_element_type=jnp.float32,
    ).astype(jnp.bfloat16)
    moe_normed = scaled_norm(moe_tokens, moe_gain)
    experts = expert_gate.shape[0] * lax.axis_size("ep")
    row_count, top_count = expert_ids.shape
    capacity = top_count * row_count // experts + max(1, top_count * row_count // (8 * experts))
    width_model = moe_tokens.shape[1]
    flat_ids = expert_ids.reshape(-1)
    onehot = (flat_ids[:, None] == jnp.arange(experts, dtype=jnp.int32)[None, :]).astype(jnp.int32)
    slot_rank = jnp.sum((jnp.cumsum(onehot, axis=0) - onehot) * onehot, axis=1)
    slot_index = flat_ids * capacity + slot_rank
    slot_match = slot_index[:, None] == jnp.arange(experts * capacity, dtype=jnp.int32)[None, :]
    dispatch_map = jnp.any(
        slot_match.reshape(row_count, top_count, experts * capacity), axis=1
    ).astype(jnp.bfloat16)
    outgoing = lax.dot_general(
        dispatch_map, moe_normed, (((0,), (0,)), ((), ())), preferred_element_type=jnp.float32
    ).astype(jnp.bfloat16)
    arrived = lax.all_to_all(
        outgoing.reshape(experts, capacity, width_model),
        "ep",
        split_axis=0,
        concat_axis=0,
        tiled=True,
    )
    arrived_rows = arrived.reshape(-1, width_model)
    w_gate = expert_gate[0]
    w_up = expert_up[0]
    w_down = expert_down[0]
    portion = lax.all_gather(arrived_rows, "tp", axis=0, tiled=True)
    gate_value = jnp.dot(portion, w_gate, preferred_element_type=jnp.float32)
    up_value = jnp.dot(portion, w_up, preferred_element_type=jnp.float32)
    hidden = (jax.nn.silu(gate_value) * up_value).astype(jnp.bfloat16)
    summed = lax.psum_scatter(
        jnp.dot(hidden, w_down, preferred_element_type=jnp.float32).astype(jnp.bfloat16),
        "tp",
        scatter_dimension=0,
        tiled=True,
    )
    returned = lax.all_to_all(
        summed.reshape(experts, capacity, width_model),
        "ep",
        split_axis=0,
        concat_axis=0,
        tiled=True,
    )
    flat_back = returned.reshape(experts * capacity, width_model)
    picked = flat_back[slot_index].reshape(row_count, top_count, width_model)
    route_weight = jax.nn.softmax(expert_scores, axis=1)
    moe_out = jnp.sum(route_weight[:, :, None] * picked.astype(jnp.float32), axis=1).astype(
        jnp.bfloat16
    )
    return (mix_out, moe_out)


def solution(mesh):
    in_specs = (
        P(("ep", "tp"), None),
        P(),
        P(None, "tp"),
        P(None, "tp"),
        P(None, "tp"),
        P(None, "tp"),
        P("tp", None),
        P(("ep", "tp"), None),
        P(),
        P(("ep", "tp"), None),
        P(("ep", "tp"), None),
        P("ep", None, "tp"),
        P("ep", None, "tp"),
        P("ep", "tp", None),
    )
    out_specs = (P(("ep", "tp"), None), P(("ep", "tp"), None))
    return jax.shard_map(shards, mesh=mesh, in_specs=in_specs, out_specs=out_specs, check_vma=False)
```

profile of v0, /device:TPU:1, one launch (start us, length us, event | category | flops | bytes accessed | tf_op | source)
XLA Modules:
  0.0 292.0 jit_solution(8549273080741177627)
XLA Ops:
  7.2 0.8 copy.25
  9.0 0.7 convert_element_type.89
  9.7 1.1 fusion.15
  10.8 1.3 convolution_convert_fusion.2
  12.4 23.4 %all_to_all.29 = bf16[16,9,2048]{2,1,0:T(8,128)(2,1)S(1)} all-to-all(bf16[16,9,2048]{2,1,0:T(8,128)(2,1)S(1)} %reshape.87), channel_id=1, replica_groups=mesh['ep'=16,'tp'=16] {'ep'}, dimensions={0} | all-to-all | bytes 1179648 | tf_op jit(solution)/shard_map/all_to_all | solution.py:82
  35.8 1.1 reshape.88
  37.2 1.0 fusion.4
  38.3 60.5 %all-gather.8.cloned.1.call-done = bf16[2304,2048]{1,0:T(8,128)(2,1)} async-done(((bf16[144,2048]{1,0:T(8,128)(2,1)}), bf16[2304,2048]{1,0:T(8,128)(2,1)}) %all-gather.8.cloned.1.call-update) | async-done | bytes 9437200 | tf_op jit(solution)/shard_map/all_gather | solution.py:93
  98.7 7.7 %fusion.8 = f32[2304,256]{1,0:T(8,128)} fusion(bf16[2304,2048]{1,0:T(8,128)(2,1)} %all-gather.8.cloned.1.call-done, bf16[1,2048,256]{2,1,0:T(8,128)(2,1)S(1)} %copy-done.5), kind=kOutput, calls=%fused_computation.15 | convolution fusion | flops 2415919104 | bytes 12845056 | tf_op jit(solution)/shard_map/dot_general | solution.py:94
  106.5 14.9 %convolution_convert_fusion = bf16[2304,2048]{1,0:T(8,128)(2,1)} fusion(bf16[2304,2048]{1,0:T(8,128)(2,1)} %all-gather.8.cloned.1.call-done, f32[2304,256]{1,0:T(8,128)} %fusion.8, bf16[1,256,2048]{2,1,0:T(8,128)(2,1)S(1)} %copy-done, bf16[1,2048,256]{2,1,0:T(8,128)(2,1)} %param.26), kind=kOutput, calls=%fused_computation.1 | convolution fusion | flops 4840095744 | bytes 23330816 | tf_op jit(solution)/shard_map/dot_general | solution.py:98
  122.1 33.5 %all-gather.4.cloned.1.call-done = bf16[2048,2048]{1,0:T(8,128)(2,1)} async-done(((bf16[128,2048]{1,0:T(8,128)(2,1)}), bf16[2048,2048]{1,0:T(8,128)(2,1)}) %all-gather.4.cloned.1.call-update) | async-done | bytes 8388624 | tf_op jit(solution)/shard_map/all_gather | solution.py:40
  155.6 6.3 %convolution_convert_fusion.1 = bf16[2048,192]{0,1:T(8,128)(2,1)S(1)} fusion(bf16[2048,2048]{1,0:T(8,128)(2,1)} %all-gather.4.cloned.1.call-done, bf16[2048,64]{0,1:T(8,128)(2,1)S(1)} %copy-done.6, bf16[2048,64]{0,1:T(8,128)(2,1)S(1)} %copy-done.7, bf16[2048,64]{0,1:T(8,128)(2,1)S(1)} %copy-done.8), kind=kOutput, calls=%fused_computation.4 | convolution fusion | flops 1613365248 | bytes 9961472 | tf_op jit(solution)/shard_map/dot_general | solution.py:39
  162.0 3.1 %collective-permute-start = (bf16[2,64]{0,1:T(8,128)(2,1)S(1)}, bf16[2,64]{0,1:T(8,128)(2,1)S(1)}, u32[]{:S(2)}, u32[]{:S(2)}) collective-permute-start(bf16[2,64]{0,1:T(8,128)(2,1)S(1)} %slice.41), channel_id=1, source_target_pairs={{0,16},{16,32},{32,48},{48,64},{64,80},{80,96},{96,112},{112,128},... | collective-permute-start | bytes 776 | tf_op jit(solution)/shard_map/ppermute | solution.py:12
  165.1 0.8 collective-permute-done
  166.0 1.0 copy_bitcast_fusion
  167.0 5.4 %all-to-all-start = ((bf16[16,128,64]{1,2,0:T(8,128)(2,1)}), bf16[16,128,64]{1,2,0:T(8,128)(2,1)S(1)}, u32[]{:S(2)}, u32[]{:S(2)}) async-start(bf16[16,128,64]{1,2,0:T(8,128)(2,1)} %copy_bitcast_fusion), calls=%async_computation | async-start | bytes 524288 | tf_op jit(solution)/shard_map/all_to_all | solution.py:60
  172.6 58.9 %reduce-scatter.2.cloned.1.call-done = bf16[144,2048]{1,0:T(8,128)(2,1)} async-done(((bf16[2304,2048]{1,0:T(8,128)(2,1)}), bf16[144,2048]{1,0:T(8,128)(2,1)}) %reduce-scatter.2.cloned.1.call-update) | async-done | bytes 589840 | tf_op jit(solution)/shard_map/reduce_scatter | solution.py:97
  231.5 2.3 reshape.89
  233.8 7.2 %all-to-all-start.2 = ((bf16[16,9,2048]{2,1,0:T(8,128)(2,1)}), bf16[16,9,2048]{2,1,0:T(8,128)(2,1)S(1)}, u32[]{:S(2)}, u32[]{:S(2)}) async-start(bf16[16,9,2048]{2,1,0:T(8,128)(2,1)} %reshape.89), calls=%async_computation.3 | async-start | bytes 2097152 | tf_op jit(solution)/shard_map/all_to_all | solution.py:103
  241.1 36.6 %all-gather.6.cloned.1.call-done = bf16[1024,2048]{1,0:T(8,128)(2,1)} async-done(((bf16[64,2048]{1,0:T(8,128)(2,1)}), bf16[1024,2048]{1,0:T(8,128)(2,1)}) %all-gather.6.cloned.1.call-update) | async-done | bytes 4194320 | tf_op jit(solution)/shard_map/all_gather | solution.py:63
  277.7 3.7 %convolution_convert_fusion.3 = bf16[128,2048]{1,0:T(8,128)(2,1)} fusion(bf16[128,1024]{0,1:T(8,128)(2,1)S(1)} %bitcast.36, bf16[1024,2048]{1,0:T(8,128)(2,1)} %all-gather.6.cloned.1.call-done), kind=kOutput, calls=%fused_computation.6 | convolution fusion | flops 537133056 | bytes 4980736 | tf_op jit(solution)/shard_map/dot_general | solution.py:61
  281.6 0.9 gather_fusion
  282.6 0.7 reshape.91
  283.2 2.2 multiply_reduce_fusion
  (53 shorter events, 2.9 us)
Async XLA Ops:
  7.2 99.3 %copy-start = (bf16[1,256,2048]{2,1,0:T(8,128)(2,1)S(1)}, bf16[1,256,2048]{2,1,0:T(8,128)(2,1)}, u32[]{:S(2)}) copy-start(bf16[1,256,2048]{2,1,0:T(8,128)(2,1)} %param.27) | copy-start | bytes 3145732
  7.2 91.6 %all-gather.8.cloned.1.call-start = ((), (), s32[]{:S(2)}) async-start(), calls=%async_computation.6 | async-start | bytes 10027008 | tf_op jit(solution)/shard_map/all_gather | solution.py:93
  12.4 24.6 %copy-start.3 = (bf16[2048]{0:T(1024)(128)(2,1)S(1)}, bf16[2048]{0:T(1024)(128)(2,1)}, u32[]{:S(2)}) copy-start(bf16[2048]{0:T(1024)(128)(2,1)} %param.15) | copy-start | bytes 12292
  35.8 1.2 copy-start.1
  36.9 61.8 %copy-start.5 = (bf16[1,2048,256]{2,1,0:T(8,128)(2,1)S(1)}, bf16[1,2048,256]{2,1,0:T(8,128)(2,1)}, u32[]{:S(2)}) copy-start(bf16[1,2048,256]{2,1,0:T(8,128)(2,1)} %param.25) | copy-start | bytes 3145732
  36.9 118.6 %all-gather.4.cloned.1.call-start = ((), (), s32[]{:S(2)}) async-start(), calls=%async_computation.4 | async-start | bytes 8912896 | tf_op jit(solution)/shard_map/all_gather | solution.py:40
  38.2 193.3 %reduce-scatter.2.cloned.1.call-start = ((), (), s32[]{:S(2)}) async-start(), calls=%async_computation.7 | async-start | bytes 10027008 | tf_op jit(solution)/shard_map/reduce_scatter | solution.py:97
  121.4 0.7 copy-start.4
  121.4 34.2 %copy-start.6 = (bf16[2048,64]{0,1:T(8,128)(2,1)S(1)}, bf16[2048,64]{0,1:T(8,128)(2,1)}, u32[]{:S(2)}) copy-start(bf16[2048,64]{0,1:T(8,128)(2,1)} %param.18) | copy-start | bytes 786436
  121.4 34.2 %copy-start.7 = (bf16[2048,64]{0,1:T(8,128)(2,1)S(1)}, bf16[2048,64]{0,1:T(8,128)(2,1)}, u32[]{:S(2)}) copy-start(bf16[2048,64]{0,1:T(8,128)(2,1)} %param.17) | copy-start | bytes 786436
  121.4 34.2 %copy-start.8 = (bf16[2048,64]{0,1:T(8,128)(2,1)S(1)}, bf16[2048,64]{0,1:T(8,128)(2,1)}, u32[]{:S(2)}) copy-start(bf16[2048,64]{0,1:T(8,128)(2,1)} %param.16) | copy-start | bytes 786436
  121.4 156.2 %all-gather.6.cloned.1.call-start = ((), (), s32[]{:S(2)}) async-start(), calls=%async_computation.5 | async-start | bytes 4456448 | tf_op jit(solution)/shard_map/all_gather | solution.py:63
  122.1 50.5 %copy-start.2 = (f32[64,2]{0,1:T(2,128)S(1)}, f32[64,2]{0,1:T(2,128)}, u32[]{:S(2)}) copy-start(f32[64,2]{0,1:T(2,128)} %param.24) | copy-start | bytes 1540
  162.0 3.9 %collective-permute-start = (bf16[2,64]{0,1:T(8,128)(2,1)S(1)}, bf16[2,64]{0,1:T(8,128)(2,1)S(1)}, u32[]{:S(2)}, u32[]{:S(2)}) collective-permute-start(bf16[2,64]{0,1:T(8,128)(2,1)S(1)} %slice.41), channel_id=1, source_target_pairs={{0,16},{16,32},{32,48},{48,64},{64,80},{80,96},{96,112},{112,128},... | collective-permute-start | bytes 776 | tf_op jit(solution)/shard_map/ppermute | solution.py:12
  167.0 66.8 %all-to-all-start = ((bf16[16,128,64]{1,2,0:T(8,128)(2,1)}), bf16[16,128,64]{1,2,0:T(8,128)(2,1)S(1)}, u32[]{:S(2)}, u32[]{:S(2)}) async-start(bf16[16,128,64]{1,2,0:T(8,128)(2,1)} %copy_bitcast_fusion), calls=%async_computation | async-start | bytes 524288 | tf_op jit(solution)/shard_map/all_to_all | solution.py:60
  233.8 47.6 %all-to-all-start.2 = ((bf16[16,9,2048]{2,1,0:T(8,128)(2,1)}), bf16[16,9,2048]{2,1,0:T(8,128)(2,1)S(1)}, u32[]{:S(2)}, u32[]{:S(2)}) async-start(bf16[16,9,2048]{2,1,0:T(8,128)(2,1)} %reshape.89), calls=%async_computation.3 | async-start | bytes 2097152 | tf_op jit(solution)/shard_map/all_to_all | solution.py:103
Sparse Core Ops, SparseCore 0:
  37.0 61.6 all-gather.7
  101.1 54.3 all-gather.3
  158.1 73.3 reduce-scatter.1
  233.2 44.4 all-gather.5
where the time goes:
time: 293 us; the launch traced here: 292 us
  waiting for transfers between devices  191 us (65%)
  matrix products  34 us (12%)
  blocking collectives  23.4 us (8%)
  starting transfers between devices  15.8 us (5%)
  between operations  14 us (5%)
  local copies, waits for them, and re-layouts  7.02 us (2%)
  other arithmetic  6.89 us (2%)
    all_gather x1, waiting for transfers between devices, shards(): portion = lax.all_gather(arrived_rows, 'tp', axis=0, tiled=True)  60.5 us
    reduce_scatter x1, waiting for transfers between devices, shards(): lax.psum_scatter(jnp.dot(hidden, w_down, preferred_element_type=jnp.float...  58.9 us
    all_gather x1, waiting for transfers between devices, shards(): lax.all_gather(out_proj, 'tp', axis=0, tiled=True)  36.6 us
    all_gather x1, waiting for transfers between devices, shards(): lax.all_gather(normed, 'tp', axis=0, tiled=True)  33.5 us
    all_to_all x1, blocking collectives, shards(): lax.all_to_all(outgoing.reshape(experts, capacity, width_model), 'ep', sp...  23.4 us
    dot_general x1, matrix products, shards(): jnp.dot(hidden, w_down, preferred_element_type=jnp.float32)  14.9 us
    dot_general x1, matrix products, shards(): gate_value = jnp.dot(portion, w_gate, preferred_element_type=jnp.float32)  7.71 us
    all_to_all x1, starting transfers between devices, shards(): lax.all_to_all(summed.reshape(experts, capacity, width_model), 'ep', spli...  7.19 us
  transfers between devices with their start and end apart: 7, of which 5 were waited for; matrix products, arithmetic and copies ran while one was open for 13% of the time, Pallas kernels for 0%

commit v1 on v0

--- a/solution.py
+++ b/solution.py
@@ -4,6 +4,19 @@
 from jax.sharding import PartitionSpec as P
 
 norm_eps = 1e-06
+
+
+def ring_gather(value, axis, dim):
+    ways = lax.axis_size(axis)
+    up = [(d, (d + 1) % ways) for d in range(ways)]
+    down = [(d, (d - 1) % ways) for d in range(ways)]
+    earlier, later = ([value], [value])
+    for _ in range(ways // 2):
+        earlier.append(lax.ppermute(earlier[-1], axis, up))
+    for _ in range((ways - 1) // 2):
+        later.append(lax.ppermute(later[-1], axis, down))
+    line = jnp.concatenate([*earlier[::-1], *later[1:]], axis=dim)
+    return jnp.roll(line, (lax.axis_index(axis) - ways // 2) * value.shape[dim], axis=dim)
 
 
 def from_behind(value, axis, steps):
@@ -59,9 +72,7 @@
     carried = (out_gate.astype(jnp.float32) * convolved).astype(jnp.bfloat16)
     token_major = lax.all_to_all(carried, "tp", split_axis=0, concat_axis=1, tiled=True)
     mix_out = jnp.dot(
-        token_major,
-        lax.all_gather(out_proj, "tp", axis=0, tiled=True),
-        preferred_element_type=jnp.float32,
+        token_major, ring_gather(out_proj, "tp", 0), preferred_element_type=jnp.float32
     ).astype(jnp.bfloat16)
     moe_normed = scaled_norm(moe_tokens, moe_gain)
     experts = expert_gate.shape[0] * lax.axis_size("ep")

time: 293 us -> 298 us (1.017)
  waiting for transfers between devices: 191 us -> 105 us
  starting transfers between devices: 15.8 us -> 68.9 us
  local copies, waits for them, and re-layouts: 7.02 us -> 41.5 us
    reduce_scatter x1, waiting for transfers between devices: 58.9 us -> 0.01 us  [shards(): lax.psum_scatter(jnp.dot(hidden, w_down, preferred_element_type=jnp.float...]
    ppermute x0 -> x15, starting transfers between devices: none -> 44.5 us  [the longest x7 32.7 us: ring_gather(): later.append(lax.ppermute(later[-1], axis, down))]
    all_gather x1 -> x0, waiting for transfers between devices: 36.6 us -> none  [shards(): lax.all_gather(out_proj, 'tp', axis=0, tiled=True)]
    unnamed x19 -> x50, local copies, waits for them, and re-layouts: 0.94 us -> 34.7 us
    all_gather x1, waiting for transfers between devices: 33.5 us -> 0.01 us  [shards(): lax.all_gather(normed, 'tp', axis=0, tiled=True)]
    ppermute x0 -> x15, waiting for transfers between devices: none -> 27.2 us  [the longest x8 26.3 us: ring_gather(): earlier.append(lax.ppermute(earlier[-1], axis, up))]
    all_to_all x1, waiting for transfers between devices: 0.01 us -> 14 us  [shards(): lax.all_to_all(summed.reshape(experts, capacity, width_model), 'ep', spli...]
    all_to_all x1, starting transfers between devices: 5.41 us -> 14 us  [shards(): lax.all_to_all(carried, 'tp', split_axis=0, concat_axis=1, tiled=True)]
  transfers between devices with their start and end apart: 7 -> 21, of which waited for: 5 -> 14; matrix products, arithmetic and copies ran while one was open for 13% -> 25% of each run, Pallas kernels for 0% -> 0%
where the time goes in v1:
time: 298 us; the launch traced here: 297 us
  waiting for transfers between devices  105 us (35%)
  starting transfers between devices  68.9 us (23%)
  local copies, waits for them, and re-layouts  41.5 us (14%)
  matrix products  34.2 us (11%)
  blocking collectives  23.4 us (8%)
  between operations  14 us (5%)
  other arithmetic  9.65 us (3%)
    all_gather x1, waiting for transfers between devices, shards(): portion = lax.all_gather(arrived_rows, 'tp', axis=0, tiled=True)  57.7 us
    unnamed x50, local copies, waits for them, and re-layouts  34.7 us
    ppermute x7, starting transfers between devices, ring_gather(): later.append(lax.ppermute(later[-1], axis, down))  32.7 us
    ppermute x8, waiting for transfers between devices, ring_gather(): earlier.append(lax.ppermute(earlier[-1], axis, up))  26.3 us
    all_to_all x1, blocking collectives, shards(): lax.all_to_all(outgoing.reshape(experts, capacity, width_model), 'ep', sp...  23.4 us
    dot_general x1, matrix products, shards(): jnp.dot(hidden, w_down, preferred_element_type=jnp.float32)  14.6 us
    all_to_all x1, waiting for transfers between devices, shards(): lax.all_to_all(summed.reshape(experts, capacity, width_model), 'ep', spli...  14 us
    all_to_all x1, starting transfers between devices, shards(): lax.all_to_all(carried, 'tp', split_axis=0, concat_axis=1, tiled=True)  14 us
  transfers between devices with their start and end apart: 21, of which 14 were waited for; matrix products, arithmetic and copies ran while one was open for 25% of the time, Pallas kernels for 0%

profile of v1, /device:TPU:1, one launch (start us, length us, event | category | flops | bytes accessed | tf_op | source)
XLA Modules:
  0.0 297.0 jit_solution(3866462380588941624)
XLA Ops:
  12.4 23.4 %all_to_all.29 = bf16[16,9,2048]{2,1,0:T(8,128)(2,1)S(1)} all-to-all(bf16[16,9,2048]{2,1,0:T(8,128)(2,1)S(1)} %reshape.87), channel_id=1, replica_groups=mesh['ep'=16,'tp'=16] {'ep'}, dimensions={0} | all-to-all | bytes 1179648 | tf_op jit(solution)/shard_map/all_to_all | solution.py:93
  41.0 57.7 %all-gather.5.cloned.1.call-done = bf16[2304,2048]{1,0:T(8,128)(2,1)} async-done(((bf16[144,2048]{1,0:T(8,128)(2,1)}), bf16[2304,2048]{1,0:T(8,128)(2,1)}) %all-gather.5.cloned.1.call-update) | async-done | bytes 9437200 | tf_op jit(solution)/shard_map/all_gather | solution.py:104
  98.7 8.0 %fusion.13 = f32[2304,256]{1,0:T(8,128)} fusion(bf16[2304,2048]{1,0:T(8,128)(2,1)} %all-gather.5.cloned.1.call-done, bf16[1,2048,256]{2,1,0:T(8,128)(2,1)} %param.25), kind=kOutput, calls=%fused_computation.17 | convolution fusion | flops 2415919104 | bytes 12845056 | tf_op jit(solution)/shard_map/dot_general | solution.py:105
  106.7 14.6 %convolution_convert_fusion = bf16[2304,2048]{1,0:T(8,128)(2,1)} fusion(bf16[2304,2048]{1,0:T(8,128)(2,1)} %all-gather.5.cloned.1.call-done, f32[2304,256]{1,0:T(8,128)} %fusion.13, bf16[1,256,2048]{2,1,0:T(8,128)(2,1)S(1)} %copy-done, bf16[1,2048,256]{2,1,0:T(8,128)(2,1)S(1)} %copy-done.8), kind=kOutput, calls=%fused_computation.1 | convolution fusion | flops 4840095744 | bytes 23330816 | tf_op jit(solution)/shard_map/dot_general | solution.py:109
  122.3 8.9 %collective-permute-done.1 = bf16[64,2048]{1,0:T(8,128)(2,1)S(1)} collective-permute-done((bf16[64,2048]{1,0:T(8,128)(2,1)S(1)}, bf16[64,2048]{1,0:T(8,128)(2,1)S(1)}, u32[]{:S(2)}, u32[]{:S(2)}) %collective-permute-start.1) | collective-permute-done | bytes 262176 | tf_op jit(solution)/shard_map/ppermute | solution.py:15
  131.2 2.5 collective-permute-start.2
  135.3 7.4 %collective-permute-done.2 = bf16[64,2048]{1,0:T(8,128)(2,1)S(1)} collective-permute-done((bf16[64,2048]{1,0:T(8,128)(2,1)S(1)}, bf16[64,2048]{1,0:T(8,128)(2,1)S(1)}, u32[]{:S(2)}, u32[]{:S(2)}) %collective-permute-start.2) | collective-permute-done | bytes 262176 | tf_op jit(solution)/shard_map/ppermute | solution.py:15
  142.7 2.5 collective-permute-start.3
  145.2 2.9 collective-permute-start.10
  148.1 6.2 %collective-permute-done.3 = bf16[64,2048]{1,0:T(8,128)(2,1)S(1)} collective-permute-done((bf16[64,2048]{1,0:T(8,128)(2,1)S(1)}, bf16[64,2048]{1,0:T(8,128)(2,1)S(1)}, u32[]{:S(2)}, u32[]{:S(2)}) %collective-permute-start.3) | collective-permute-done | bytes 262176 | tf_op jit(solution)/shard_map/ppermute | solution.py:15
  154.2 2.5 collective-permute-start.4
  156.9 3.9 %collective-permute-start.11 = (bf16[64,2048]{1,0:T(8,128)(2,1)S(1)}, bf16[64,2048]{1,0:T(8,128)(2,1)S(1)}, u32[]{:S(2)}, u32[]{:S(2)}) collective-permute-start(bf16[64,2048]{1,0:T(8,128)(2,1)S(1)} %collective-permute-done.10), channel_id=1, source_target_pairs={{0,15},{1,0},{2,1},{3,2},{4,3},{5,4},{6,5},{7,6},{8,7},{9,8},{10,9... | collective-permute-start | bytes 786440 | tf_op jit(solution)/shard_map/ppermute | solution.py:17
  161.8 2.4 collective-permute-start.5
  164.3 3.6 %collective-permute-start.12 = (bf16[64,2048]{1,0:T(8,128)(2,1)S(1)}, bf16[64,2048]{1,0:T(8,128)(2,1)S(1)}, u32[]{:S(2)}, u32[]{:S(2)}) collective-permute-start(bf16[64,2048]{1,0:T(8,128)(2,1)S(1)} %collective-permute-done.11), channel_id=1, source_target_pairs={{0,15},{1,0},{2,1},{3,2},{4,3},{5,4},{6,5},{7,6},{8,7},{9,8},{10,9... | collective-permute-start | bytes 786440 | tf_op jit(solution)/shard_map/ppermute | solution.py:17
  170.4 4.8 %collective-permute-start.13 = (bf16[64,2048]{1,0:T(8,128)(2,1)S(1)}, bf16[64,2048]{1,0:T(8,128)(2,1)}, u32[]{:S(2)}, u32[]{:S(2)}) collective-permute-start(bf16[64,2048]{1,0:T(8,128)(2,1)S(1)} %collective-permute-done.12), channel_id=1, source_target_pairs={{0,15},{1,0},{2,1},{3,2},{4,3},{5,4},{6,5},{7,6},{8,7},{9,8},{10,9... | collective-permute-start | bytes 786440 | tf_op jit(solution)/shard_map/ppermute | solution.py:17
  176.4 8.0 %collective-permute-start.14 = (bf16[64,2048]{1,0:T(8,128)(2,1)}, bf16[64,2048]{1,0:T(8,128)(2,1)S(1)}, u32[]{:S(2)}, u32[]{:S(2)}) collective-permute-start(bf16[64,2048]{1,0:T(8,128)(2,1)} %collective-permute-done.13), channel_id=1, source_target_pairs={{0,15},{1,0},{2,1},{3,2},{4,3},{5,4},{6,5},{7,6},{8,7},{9,8},{10,9... | collective-permute-start | bytes 786440 | tf_op jit(solution)/shard_map/ppermute | solution.py:17
  185.8 7.9 %collective-permute-start.15 = (bf16[64,2048]{1,0:T(8,128)(2,1)S(1)}, bf16[64,2048]{1,0:T(8,128)(2,1)S(1)}, u32[]{:S(2)}, u32[]{:S(2)}) collective-permute-start(bf16[64,2048]{1,0:T(8,128)(2,1)S(1)} %collective-permute-done.14), channel_id=1, source_target_pairs={{0,15},{1,0},{2,1},{3,2},{4,3},{5,4},{6,5},{7,6},{8,7},{9,8},{10,9... | collective-permute-start | bytes 786440 | tf_op jit(solution)/shard_map/ppermute | solution.py:17
  222.8 6.6 %convolution_convert_fusion.1 = bf16[2048,192]{0,1:T(8,128)(2,1)S(1)} fusion(bf16[2048,2048]{1,0:T(8,128)(2,1)} %all-gather.3.cloned.1.call-done, bf16[2048,64]{0,1:T(8,128)(2,1)} %param.18, bf16[2048,64]{0,1:T(8,128)(2,1)} %param.17, bf16[2048,64]{0,1:T(8,128)(2,1)} %param.16), kind=kOutput, calls=%fused_computation.6 | convolution fusion | flops 1613365248 | bytes 9961472 | tf_op jit(solution)/shard_map/dot_general | solution.py:52
  229.5 3.0 %collective-permute-start = (bf16[2,64]{0,1:T(8,128)(2,1)S(1)}, bf16[2,64]{0,1:T(8,128)(2,1)S(1)}, u32[]{:S(2)}, u32[]{:S(2)}) collective-permute-start(bf16[2,64]{0,1:T(8,128)(2,1)S(1)} %slice.41), channel_id=1, source_target_pairs={{0,16},{16,32},{32,48},{48,64},{64,80},{80,96},{96,112},{112,128},... | collective-permute-start | bytes 776 | tf_op jit(solution)/shard_map/ppermute | solution.py:25
  234.4 14.0 %all-to-all-start = ((bf16[16,128,64]{1,2,0:T(8,128)(2,1)}), bf16[16,128,64]{1,2,0:T(8,128)(2,1)S(1)}, u32[]{:S(2)}, u32[]{:S(2)}) async-start(bf16[16,128,64]{1,2,0:T(8,128)(2,1)} %copy_bitcast_fusion), calls=%async_computation | async-start | bytes 524288 | tf_op jit(solution)/shard_map/all_to_all | solution.py:73
  253.7 6.2 %all-to-all-done = bf16[16,128,64]{1,2,0:T(8,128)(2,1)S(1)} async-done(((bf16[16,128,64]{1,2,0:T(8,128)(2,1)}), bf16[16,128,64]{1,2,0:T(8,128)(2,1)S(1)}, u32[]{:S(2)}, u32[]{:S(2)}) %all-to-all-start) | async-done | bytes 262176 | tf_op jit(solution)/shard_map/all_to_all | solution.py:73
  259.9 7.3 %all-to-all-start.2 = ((bf16[16,9,2048]{2,1,0:T(8,128)(2,1)}), bf16[16,9,2048]{2,1,0:T(8,128)(2,1)S(1)}, u32[]{:S(2)}, u32[]{:S(2)}) async-start(bf16[16,9,2048]{2,1,0:T(8,128)(2,1)} %reshape.89), calls=%async_computation.3 | async-start | bytes 2097152 | tf_op jit(solution)/shard_map/all_to_all | solution.py:114
  268.7 3.7 %fusion.3 = bf16[128,2048]{1,0:T(8,128)(2,1)} fusion(bf16[128,1024]{0,1:T(8,128)(2,1)S(1)} %bitcast.35, bf16[2048,2048]{1,0:T(8,128)(2,1)} %constant_dynamic-update-slice_fusion, s32[]{:T(128)S(6)} %select_n.24), kind=kOutput, calls=%fused_computation.8 | convolution fusion | flops 537133056 | bytes 4980740 | tf_op jit(solution)/shard_map/dot_general | solution.py:74
  272.4 14.0 %all-to-all-done.2 = bf16[16,9,2048]{2,1,0:T(8,128)(2,1)S(1)} async-done(((bf16[16,9,2048]{2,1,0:T(8,128)(2,1)}), bf16[16,9,2048]{2,1,0:T(8,128)(2,1)S(1)}, u32[]{:S(2)}, u32[]{:S(2)}) %all-to-all-start.2) | async-done | bytes 589856 | tf_op jit(solution)/shard_map/all_to_all | solution.py:114
  (112 shorter events, 61.1 us)
Async XLA Ops:
  7.2 99.5 %copy-start = (bf16[1,256,2048]{2,1,0:T(8,128)(2,1)S(1)}, bf16[1,256,2048]{2,1,0:T(8,128)(2,1)}, u32[]{:S(2)}) copy-start(bf16[1,256,2048]{2,1,0:T(8,128)(2,1)} %param.27) | copy-start | bytes 3145732
  7.2 91.5 %all-gather.5.cloned.1.call-start = ((), (), s32[]{:S(2)}) async-start(), calls=%async_computation.5 | async-start | bytes 10027008 | tf_op jit(solution)/shard_map/all_gather | solution.py:104
  36.9 185.9 %all-gather.3.cloned.1.call-start = ((), (), s32[]{:S(2)}) async-start(), calls=%async_computation.4 | async-start | bytes 8912896 | tf_op jit(solution)/shard_map/all_gather | solution.py:53
  40.9 65.7 %copy-start.8 = (bf16[1,2048,256]{2,1,0:T(8,128)(2,1)S(1)}, bf16[1,2048,256]{2,1,0:T(8,128)(2,1)}, u32[]{:S(2)}) copy-start(bf16[1,2048,256]{2,1,0:T(8,128)(2,1)} %param.26) | copy-start | bytes 3145732
  41.0 210.4 %reduce-scatter.2.cloned.1.call-start = ((), (), s32[]{:S(2)}) async-start(), calls=%async_computation.6 | async-start | bytes 10027008 | tf_op jit(solution)/shard_map/reduce_scatter | solution.py:108
  121.3 63.8 %copy-start.7 = (bf16[3,64]{1,0:T(4,128)(2,1)S(1)}, bf16[3,64]{1,0:T(4,128)(2,1)}, u32[]{:S(2)}) copy-start(bf16[3,64]{1,0:T(4,128)(2,1)} %param.19) | copy-start | bytes 1156
  122.3 8.9 %collective-permute-start.1 = (bf16[64,2048]{1,0:T(8,128)(2,1)S(1)}, bf16[64,2048]{1,0:T(8,128)(2,1)S(1)}, u32[]{:S(2)}, u32[]{:S(2)}) collective-permute-start(bf16[64,2048]{1,0:T(8,128)(2,1)S(1)} %copy-done.1), channel_id=1, source_target_pairs={{0,1},{1,2},{2,3},{3,4},{4,5},{5,6},{6,7},{7,8},{8,9},{9,10},{10,1... | collective-permute-start | bytes 786440 | tf_op jit(solution)/shard_map/ppermute | solution.py:15
  131.2 11.5 %collective-permute-start.2 = (bf16[64,2048]{1,0:T(8,128)(2,1)S(1)}, bf16[64,2048]{1,0:T(8,128)(2,1)S(1)}, u32[]{:S(2)}, u32[]{:S(2)}) collective-permute-start(bf16[64,2048]{1,0:T(8,128)(2,1)S(1)} %collective-permute-done.1), channel_id=1, source_target_pairs={{0,1},{1,2},{2,3},{3,4},{4,5},{5,6},{6,7},{7,8},{8,9},{9,10},{10,1... | collective-permute-start | bytes 786440 | tf_op jit(solution)/shard_map/ppermute | solution.py:15
  133.6 11.5 %collective-permute-start.9 = (bf16[64,2048]{1,0:T(8,128)(2,1)S(1)}, bf16[64,2048]{1,0:T(8,128)(2,1)S(1)}, u32[]{:S(2)}, u32[]{:S(2)}) collective-permute-start(bf16[64,2048]{1,0:T(8,128)(2,1)S(1)} %copy-done.1), channel_id=1, source_target_pairs={{0,15},{1,0},{2,1},{3,2},{4,3},{5,4},{6,5},{7,6},{8,7},{9,8},{10,9... | collective-permute-start | bytes 786440 | tf_op jit(solution)/shard_map/ppermute | solution.py:17
  142.7 11.5 %collective-permute-start.3 = (bf16[64,2048]{1,0:T(8,128)(2,1)S(1)}, bf16[64,2048]{1,0:T(8,128)(2,1)S(1)}, u32[]{:S(2)}, u32[]{:S(2)}) collective-permute-start(bf16[64,2048]{1,0:T(8,128)(2,1)S(1)} %collective-permute-done.2), channel_id=1, source_target_pairs={{0,1},{1,2},{2,3},{3,4},{4,5},{5,6},{6,7},{7,8},{8,9},{9,10},{10,1... | collective-permute-start | bytes 786440 | tf_op jit(solution)/shard_map/ppermute | solution.py:15
  145.2 11.7 %collective-permute-start.10 = (bf16[64,2048]{1,0:T(8,128)(2,1)S(1)}, bf16[64,2048]{1,0:T(8,128)(2,1)S(1)}, u32[]{:S(2)}, u32[]{:S(2)}) collective-permute-start(bf16[64,2048]{1,0:T(8,128)(2,1)S(1)} %collective-permute-done.9), channel_id=1, source_target_pairs={{0,15},{1,0},{2,1},{3,2},{4,3},{5,4},{6,5},{7,6},{8,7},{9,8},{10,9... | collective-permute-start | bytes 786440 | tf_op jit(solution)/shard_map/ppermute | solution.py:17
  154.2 7.6 %collective-permute-start.4 = (bf16[64,2048]{1,0:T(8,128)(2,1)S(1)}, bf16[64,2048]{1,0:T(8,128)(2,1)S(1)}, u32[]{:S(2)}, u32[]{:S(2)}) collective-permute-start(bf16[64,2048]{1,0:T(8,128)(2,1)S(1)} %collective-permute-done.3), channel_id=1, source_target_pairs={{0,1},{1,2},{2,3},{3,4},{4,5},{5,6},{6,7},{7,8},{8,9},{9,10},{10,1... | collective-permute-start | bytes 786440 | tf_op jit(solution)/shard_map/ppermute | solution.py:15
  156.9 7.4 %collective-permute-start.11 = (bf16[64,2048]{1,0:T(8,128)(2,1)S(1)}, bf16[64,2048]{1,0:T(8,128)(2,1)S(1)}, u32[]{:S(2)}, u32[]{:S(2)}) collective-permute-start(bf16[64,2048]{1,0:T(8,128)(2,1)S(1)} %collective-permute-done.10), channel_id=1, source_target_pairs={{0,15},{1,0},{2,1},{3,2},{4,3},{5,4},{6,5},{7,6},{8,7},{9,8},{10,9... | collective-permute-start | bytes 786440 | tf_op jit(solution)/shard_map/ppermute | solution.py:17
  161.8 7.1 %collective-permute-start.5 = (bf16[64,2048]{1,0:T(8,128)(2,1)S(1)}, bf16[64,2048]{1,0:T(8,128)(2,1)}, u32[]{:S(2)}, u32[]{:S(2)}) collective-permute-start(bf16[64,2048]{1,0:T(8,128)(2,1)S(1)} %collective-permute-done.4), channel_id=1, source_target_pairs={{0,1},{1,2},{2,3},{3,4},{4,5},{5,6},{6,7},{7,8},{8,9},{9,10},{10,1... | collective-permute-start | bytes 786440 | tf_op jit(solution)/shard_map/ppermute | solution.py:15
  164.3 6.1 %collective-permute-start.12 = (bf16[64,2048]{1,0:T(8,128)(2,1)S(1)}, bf16[64,2048]{1,0:T(8,128)(2,1)S(1)}, u32[]{:S(2)}, u32[]{:S(2)}) collective-permute-start(bf16[64,2048]{1,0:T(8,128)(2,1)S(1)} %collective-permute-done.11), channel_id=1, source_target_pairs={{0,15},{1,0},{2,1},{3,2},{4,3},{5,4},{6,5},{7,6},{8,7},{9,8},{10,9... | collective-permute-start | bytes 786440 | tf_op jit(solution)/shard_map/ppermute | solution.py:17
  169.0 7.3 %collective-permute-start.6 = (bf16[64,2048]{1,0:T(8,128)(2,1)}, bf16[64,2048]{1,0:T(8,128)(2,1)}, u32[]{:S(2)}, u32[]{:S(2)}) collective-permute-start(bf16[64,2048]{1,0:T(8,128)(2,1)} %collective-permute-done.5), channel_id=1, source_target_pairs={{0,1},{1,2},{2,3},{3,4},{4,5},{5,6},{6,7},{7,8},{8,9},{9,10},{10,1... | collective-permute-start | bytes 786440 | tf_op jit(solution)/shard_map/ppermute | solution.py:15
  170.4 6.1 %collective-permute-start.13 = (bf16[64,2048]{1,0:T(8,128)(2,1)S(1)}, bf16[64,2048]{1,0:T(8,128)(2,1)}, u32[]{:S(2)}, u32[]{:S(2)}) collective-permute-start(bf16[64,2048]{1,0:T(8,128)(2,1)S(1)} %collective-permute-done.12), channel_id=1, source_target_pairs={{0,15},{1,0},{2,1},{3,2},{4,3},{5,4},{6,5},{7,6},{8,7},{9,8},{10,9... | collective-permute-start | bytes 786440 | tf_op jit(solution)/shard_map/ppermute | solution.py:17
  176.3 8.1 %collective-permute-start.7 = (bf16[64,2048]{1,0:T(8,128)(2,1)}, bf16[64,2048]{1,0:T(8,128)(2,1)}, u32[]{:S(2)}, u32[]{:S(2)}) collective-permute-start(bf16[64,2048]{1,0:T(8,128)(2,1)} %collective-permute-done.6), channel_id=1, source_target_pairs={{0,1},{1,2},{2,3},{3,4},{4,5},{5,6},{6,7},{7,8},{8,9},{9,10},{10,1... | collective-permute-start | bytes 786440 | tf_op jit(solution)/shard_map/ppermute | solution.py:15
  176.4 9.4 %collective-permute-start.14 = (bf16[64,2048]{1,0:T(8,128)(2,1)}, bf16[64,2048]{1,0:T(8,128)(2,1)S(1)}, u32[]{:S(2)}, u32[]{:S(2)}) collective-permute-start(bf16[64,2048]{1,0:T(8,128)(2,1)} %collective-permute-done.13), channel_id=1, source_target_pairs={{0,15},{1,0},{2,1},{3,2},{4,3},{5,4},{6,5},{7,6},{8,7},{9,8},{10,9... | collective-permute-start | bytes 786440 | tf_op jit(solution)/shard_map/ppermute | solution.py:17
  184.4 9.9 %collective-permute-start.8 = (bf16[64,2048]{1,0:T(8,128)(2,1)}, bf16[64,2048]{1,0:T(8,128)(2,1)}, u32[]{:S(2)}, u32[]{:S(2)}) collective-permute-start(bf16[64,2048]{1,0:T(8,128)(2,1)} %collective-permute-done.7), channel_id=1, source_target_pairs={{0,1},{1,2},{2,3},{3,4},{4,5},{5,6},{6,7},{7,8},{8,9},{9,10},{10,1... | collective-permute-start | bytes 786440 | tf_op jit(solution)/shard_map/ppermute | solution.py:15
  185.8 25.1 %collective-permute-start.15 = (bf16[64,2048]{1,0:T(8,128)(2,1)S(1)}, bf16[64,2048]{1,0:T(8,128)(2,1)S(1)}, u32[]{:S(2)}, u32[]{:S(2)}) collective-permute-start(bf16[64,2048]{1,0:T(8,128)(2,1)S(1)} %collective-permute-done.14), channel_id=1, source_target_pairs={{0,15},{1,0},{2,1},{3,2},{4,3},{5,4},{6,5},{7,6},{8,7},{9,8},{10,9... | collective-permute-start | bytes 786440 | tf_op jit(solution)/shard_map/ppermute | solution.py:17
  229.5 3.9 %collective-permute-start = (bf16[2,64]{0,1:T(8,128)(2,1)S(1)}, bf16[2,64]{0,1:T(8,128)(2,1)S(1)}, u32[]{:S(2)}, u32[]{:S(2)}) collective-permute-start(bf16[2,64]{0,1:T(8,128)(2,1)S(1)} %slice.41), channel_id=1, source_target_pairs={{0,16},{16,32},{32,48},{48,64},{64,80},{80,96},{96,112},{112,128},... | collective-permute-start | bytes 776 | tf_op jit(solution)/shard_map/ppermute | solution.py:25
  234.4 25.5 %all-to-all-start = ((bf16[16,128,64]{1,2,0:T(8,128)(2,1)}), bf16[16,128,64]{1,2,0:T(8,128)(2,1)S(1)}, u32[]{:S(2)}, u32[]{:S(2)}) async-start(bf16[16,128,64]{1,2,0:T(8,128)(2,1)} %copy_bitcast_fusion), calls=%async_computation | async-start | bytes 524288 | tf_op jit(solution)/shard_map/all_to_all | solution.py:73
  259.9 26.5 %all-to-all-start.2 = ((bf16[16,9,2048]{2,1,0:T(8,128)(2,1)}), bf16[16,9,2048]{2,1,0:T(8,128)(2,1)S(1)}, u32[]{:S(2)}, u32[]{:S(2)}) async-start(bf16[16,9,2048]{2,1,0:T(8,128)(2,1)} %reshape.89), calls=%async_computation.3 | async-start | bytes 2097152 | tf_op jit(solution)/shard_map/all_to_all | solution.py:114
  (6 other events, 153.9 us)
Sparse Core Ops, SparseCore 0:
  37.0 61.6 all-gather.4
  101.1 62.8 all-gather.2
  166.5 74.3 reduce-scatter.1
